TPU v7x, 32 devices: a whole 2x2x4 slice. The times are simulated.
32 devices in a mesh: fs: 8 (over z, x), tp: 4 (over y, core).
Axes of the slice: x: 2, y: 2, z: 4, core: 2. Of those that a mesh axis runs over, the one named last changes fastest.
Arguments:
- tokens: bfloat16 [8192, 2048], P('fs', 'tp'), may hold values from -50 to 50
- norm_gain: float32 [2048], P('fs'), may hold values from 0.1 to 1.9
- gate_weight: float32 [2048, 2816], P('fs', 'tp'), may hold values from -0.125 to 0.125
- up_weight: float32 [2048, 2816], P('fs', 'tp'), may hold values from -0.125 to 0.125
- down_weight: float32 [2816, 2048], P('fs', 'tp'), may hold values from -0.109375 to 0.109375
Outputs:
- gate_sampler: bfloat16 [2048, 2816], P(None, 'tp')
- up_sampler: bfloat16 [2048, 2816], P(None, 'tp')
- down_sampler: bfloat16 [2816, 2048], P('tp')
- mixed: bfloat16 [8192, 2048], P('fs', 'tp')
All inputs are finite; a program needn't handle non-finite values.
Results may differ from a plain program's by a relative error of at most 0.0095.
Values may be sent and summed in bfloat16 or wider, within the bound.
A program may use at most 128 MiB of HBM per device.

v0:
```python
import jax
import jax.numpy as jnp
from jax import lax
from jax.sharding import PartitionSpec as P

norm_eps = 1e-06


def shards(tokens, norm_gain, gate_weight, up_weight, down_weight):
    gate_local = (norm_gain[:, None] * gate_weight).astype(jnp.bfloat16)
    up_local = (norm_gain[:, None] * up_weight).astype(jnp.bfloat16)
    down_local = down_weight.astype(jnp.bfloat16)
    gathered = lax.all_gather(tokens, "tp", axis=1, tiled=True)
    floated = gathered.astype(jnp.float32)
    normed = (
        floated * lax.rsqrt(jnp.mean(floated * floated, axis=-1, keepdims=True) + norm_eps)
    ).astype(jnp.bfloat16)
    gate_sampler, up_sampler = (
        lax.all_gather(gate_local, "fs", axis=0, tiled=True),
        lax.all_gather(up_local, "fs", axis=0, tiled=True),
    )
    gate = jnp.dot(normed, gate_sampler, preferred_element_type=jnp.float32)
    up = jnp.dot(normed, up_sampler, preferred_element_type=jnp.float32)
    hidden = (jax.nn.silu(gate) * up).astype(jnp.bfloat16)
    down_columns = lax.all_gather(down_local, "fs", axis=0, tiled=True)
    down_sampler = lax.all_to_all(down_columns, "tp", split_axis=0, concat_axis=1, tiled=True)
    partial_value = jnp.dot(
        lax.all_gather(hidden, "tp", axis=1, tiled=True),
        down_columns,
        preferred_element_type=jnp.float32,
    ).astype(jnp.bfloat16)
    partial_value = lax.optimization_barrier(partial_value)
    summed = partial_value.astype(jnp.float32)
    return (gate_sampler, up_sampler, down_sampler, summed.astype(jnp.bfloat16))


def solution(mesh):
    return jax.shard_map(
        shards,
        mesh=mesh,
        in_specs=(P("fs", "tp"), P("fs"), P("fs", "tp"), P("fs", "tp"), P("fs", "tp")),
        out_specs=(P(None, "tp"), P(None, "tp"), P("tp", None), P("fs", "tp")),
        check_vma=False,
    )
```

profile of v0, /device:TPU:0, one launch (start us, length us, event | category | flops | bytes accessed | tf_op | source)
XLA Modules:
  0.0 316.4 jit_solution(10165208772231586884)
XLA Ops:
  7.2 0.0 copy-start.2
  7.2 0.0 all-gather.12.cloned.1.call-start
  7.2 0.7 all-gather.12.cloned.1.call-update
  7.9 0.0 all-gather.6.cloned.1.call-start
  8.0 2.3 multiply_convert_fusion.1
  10.3 0.0 all-gather.6.cloned.1.call-update
  10.3 0.0 all-gather.8.cloned.1.call-start
  10.3 0.7 all-gather.8.cloned.1.call-update
  11.0 0.0 all-gather.10.cloned.1.call-start
  11.1 0.0 copy-done.2
  11.1 0.8 convert_element_type.25
  11.9 0.0 all-gather.10.cloned.1.call-update
  11.9 0.0 all-gather.14.cloned.1.call-start
  11.9 34.8 %all-gather.12.cloned.1.call-done = bf16[1024,2048]{1,0:T(8,128)(2,1)} async-done(((bf16[1024,512]{1,0:T(8,128)(2,1)}), bf16[1024,2048]{1,0:T(8,128)(2,1)}) %all-gather.12.cloned.1.call-update) | async-done | bytes 4194320 | tf_op jit(solution)/shard_map/all_gather | solution.py:13
  46.8 3.1 fusion
  49.8 59.1 %all-gather.6.cloned.1.call-done = bf16[2048,704]{0,1:T(8,128)(2,1)} async-done(((bf16[256,704]{0,1:T(8,128)(2,1)}), bf16[2048,704]{0,1:T(8,128)(2,1)}) %all-gather.6.cloned.1.call-update) | async-done | bytes 2883600 | tf_op jit(solution)/shard_map/all_gather | solution.py:19
  109.0 6.3 %fusion.3 = f32[1024,704]{0,1:T(8,128)S(1)} fusion(bf16[2048,704]{0,1:T(8,128)(2,1)} %all-gather.6.cloned.1.call-done, bf16[1024,2048]{1,0:T(8,128)(2,1)} %all-gather.12.cloned.1.call-done, f32[1024]{0:T(1024)S(1)} %add_rsqrt_fusion), kind=kOutput, calls=%fused_computation.5 | convolution fusion | flops 2959081472 | bytes 9965568 | tf_op jit(solution)/shard_map/dot_general | solution.py:22
  115.2 54.1 %all-gather.8.cloned.1.call-done = bf16[2048,704]{0,1:T(8,128)(2,1)} async-done(((bf16[256,704]{0,1:T(8,128)(2,1)}), bf16[2048,704]{0,1:T(8,128)(2,1)}) %all-gather.8.cloned.1.call-update) | async-done | bytes 2883600 | tf_op jit(solution)/shard_map/all_gather | solution.py:20
  169.4 7.7 %multiply_convert_fusion = bf16[1024,704]{0,1:T(8,128)(2,1)} fusion(f32[1024,704]{0,1:T(8,128)S(1)} %fusion.3, bf16[2048,704]{0,1:T(8,128)(2,1)} %all-gather.8.cloned.1.call-done, bf16[1024,2048]{1,0:T(8,128)(2,1)} %all-gather.12.cloned.1.call-done, f32[1024]{0:T(1024)S(1)} %add_rsqrt_fusion), kind=kOutput, calls=%fused_computation.4 | convolution fusion | flops 2963406848 | bytes 11407360 | tf_op jit(solution)/shard_map/dot_general | solution.py:23
  177.1 0.0 all-gather.14.cloned.1.call-update
  177.1 50.4 %all-gather.10.cloned.1.call-done = bf16[2816,512]{1,0:T(8,128)(2,1)} async-done(((bf16[352,512]{1,0:T(8,128)(2,1)}), bf16[2816,512]{1,0:T(8,128)(2,1)}) %all-gather.10.cloned.1.call-update) | async-done | bytes 2883600 | tf_op jit(solution)/shard_map/all_gather | solution.py:25
  227.5 64.5 %all_to_all.19 = bf16[4,704,512]{2,1,0:T(8,128)(2,1)S(1)} all-to-all(bf16[4,704,512]{2,1,0:T(8,128)(2,1)} %bitcast.9), channel_id=1, replica_groups=mesh['fs'=8,'tp'=4] {'tp'}, dimensions={0} | all-to-all | bytes 5767168 | tf_op jit(solution)/shard_map/all_to_all | solution.py:26
  292.0 2.0 copy.11
  294.1 0.0 copy-start
  294.1 3.8 %all-gather.14.cloned.1.call-done = bf16[1024,2816]{0,1:T(8,128)(2,1)} async-done(((bf16[1024,704]{0,1:T(8,128)(2,1)}), bf16[1024,2816]{0,1:T(8,128)(2,1)}) %all-gather.14.cloned.1.call-update) | async-done | bytes 5767184 | tf_op jit(solution)/shard_map/all_gather | solution.py:28
  297.8 7.7 %convolution_convert_fusion = bf16[1024,512]{1,0:T(8,128)(2,1)} fusion(bf16[1024,2816]{0,1:T(8,128)(2,1)} %all-gather.14.cloned.1.call-done, bf16[2816,512]{1,0:T(8,128)(2,1)} %all-gather.10.cloned.1.call-done), kind=kOutput, calls=%fused_computation.6 | convolution fusion | flops 2953314304 | bytes 9699328 | tf_op jit(solution)/shard_map/dot_general | solution.py:27
  305.5 0.0 copy-done
  305.5 0.0 copy-start.1
  305.5 1.6 copy.14
  307.0 1.3 copy-done.1
  308.3 1.6 copy.15
  (1 shorter events, 0.0 us)
Async XLA Ops:
  7.2 3.9 %copy-start.2 = (f32[352,512]{1,0:T(8,128)S(1)}, f32[352,512]{1,0:T(8,128)}, u32[]{:S(2)}) copy-start(f32[352,512]{1,0:T(8,128)} %param.9) | copy-start | bytes 2162692
  7.2 39.6 %all-gather.12.cloned.1.call-start = ((), (), s32[]{:S(2)}) async-start(), calls=%async_computation.4 | async-start | bytes 5242880 | tf_op jit(solution)/shard_map/all_gather | solution.py:13
  7.9 101.1 %all-gather.6.cloned.1.call-start = ((), (), s32[]{:S(2)}) async-start(), calls=%async_computation.1 | async-start | bytes 3244032 | tf_op jit(solution)/shard_map/all_gather | solution.py:19
  10.3 159.1 %all-gather.8.cloned.1.call-start = ((), (), s32[]{:S(2)}) async-start(), calls=%async_computation.2 | async-start | bytes 3244032 | tf_op jit(solution)/shard_map/all_gather | solution.py:20
  11.0 216.5 %all-gather.10.cloned.1.call-start = ((), (), s32[]{:S(2)}) async-start(), calls=%async_computation.3 | async-start | bytes 3244032 | tf_op jit(solution)/shard_map/all_gather | solution.py:25
  11.9 285.9 %all-gather.14.cloned.1.call-start = ((), (), s32[]{:S(2)}) async-start(), calls=%async_computation.5 | async-start | bytes 7208960 | tf_op jit(solution)/shard_map/all_gather | solution.py:28
  294.1 11.4 %copy-start = (bf16[2048,704]{0,1:T(8,128)(2,1)S(1)}, bf16[2048,704]{0,1:T(8,128)(2,1)}, u32[]{:S(2)}) copy-start(bf16[2048,704]{0,1:T(8,128)(2,1)} %all-gather.6.cloned.1.call-done) | copy-start | bytes 8650756
  305.5 2.9 copy-start.1
Sparse Core Ops, SparseCore 0:
  9.5 37.1 all-gather.11
  49.4 59.5 all-gather.5
  111.6 57.7 all-gather.7
  172.0 55.4 all-gather.9
  229.5 68.2 all-gather.13
where the time goes:
time: 317 us; the launch traced here: 316 us
  waiting for transfers between devices  204 us (64%)
  blocking collectives  64.5 us (20%)
  matrix products  21.7 us (7%)
  between operations  13.8 us (4%)
  local copies, waits for them, and re-layouts  6.45 us (2%)
  other arithmetic  6.17 us (2%)
    all_to_all x1, blocking collectives, shards(): lax.all_to_all(down_columns, 'tp', split_axis=0, concat_axis=1, tiled=True)  64.5 us
    all_gather x1, waiting for transfers between devices, shards(): lax.all_gather(gate_local, 'fs', axis=0, tiled=True)  59.1 us
    all_gather x1, waiting for transfers between devices, shards(): lax.all_gather(up_local, 'fs', axis=0, tiled=True)  54.1 us
    all_gather x1, waiting for transfers between devices, shards(): down_columns = lax.all_gather(down_local, 'fs', axis=0, tiled=True)  50.4 us
    all_gather x1, waiting for transfers between devices, shards(): gathered = lax.all_gather(tokens, 'tp', axis=1, tiled=True)  34.8 us
    dot_general x1, matrix products, shards(): up = jnp.dot(normed, up_sampler, preferred_element_type=jnp.float32)  7.73 us
    dot_general x1, matrix products, shards(): jnp.dot(lax.all_gather(hidden, 'tp', axis=1, tiled=True), down_columns, p...  7.65 us
  transfers between devices with their start and end apart: 5, of which 5 were waited for; matrix products, arithmetic and copies ran while one was open for 7% of the time, Pallas kernels for 0%

commit v1 on v0

v1 whole, which is shorter than its diff:
```python
import functools

import jax
import jax.numpy as jnp
from jax import lax
from jax.experimental import pallas as pl
from jax.experimental.pallas import tpu as pltpu
from jax.sharding import PartitionSpec as P

norm_eps = 1e-06
MESH = pl.DeviceIdType.MESH
PIECES = 2
NT = (((1,), (1,)), ((), ()))


def remote(src, dst, send, recv, device):
    return pltpu.make_async_remote_copy(
        src_ref=src, dst_ref=dst, send_sem=send, recv_sem=recv, device_id=device, device_id_type=MESH
    )


def layer_kernel(
    lines, tp,
    tok_in, gate_in, up_in, down_in,
    gate_out, up_out, down_out, mixed_out,
    tok, normed, gu, hidden, down, part, got,
    gu_recv, gu_line, gu_pair, down_recv, down_line, down_pair, down_first,
    tok_recv, tok_send, sum_recv, sum_send, local, stored,
):
    f, t = lax.axis_index("fs"), lax.axis_index("tp")
    z, x = f // 2, f % 2
    sibling = t + 1 - 2 * (t % 2)
    across = (t + 2) % 4
    gu_in, gu_out = (gate_in, up_in), (gate_out, up_out)
    depth = gate_in.shape[1]
    down_rows, width = down_in.shape
    n_tok = tok_in.shape[0]
    tile = n_tok // tp
    pair_dev = {"fs": 2 * z + 1 - x}
    away = jnp.maximum(z - t, t - z)

    def column(k):
        return 2 * ((t // 2 + 1 - k // 2) % 2) + (t % 2 + 1 - k % 2) % 2

    barrier = pltpu.get_barrier_semaphore()
    for other in range(1, tp):
        pl.semaphore_signal(barrier, inc=1, device_id={"tp": (t + other) % tp}, device_id_type=MESH)
    pl.semaphore_signal(barrier, inc=1, device_id=pair_dev, device_id_type=MESH)

    @pl.when(z > 0)
    def _():
        pl.semaphore_signal(barrier, inc=1, device_id={"fs": f - 2}, device_id_type=MESH)

    @pl.when(z < lines - 1)
    def _():
        pl.semaphore_signal(barrier, inc=1, device_id={"fs": f + 2}, device_id_type=MESH)

    pl.semaphore_wait(barrier, tp + jnp.minimum(z, 1) + jnp.minimum(lines - 1 - z, 1))

    def gu_slot(block, p):
        return gu.at[block, p]

    def gu_source(step, block, p):
        return gu_in[p] if step == 0 else gu_slot(block, p)

    def line_copy(step, p, up):
        block = 2 * (z - step if up else z + step) + x
        return remote(
            gu_source(step, block, p), gu_slot(block, p), gu_line.at[0 if up else 1, step, p],
            gu_recv.at[block, p], {"fs": f + 2 if up else f - 2},
        )

    def pair_copy(step, level, p):
        block = 2 * level + x
        return remote(gu_source(step, block, p), gu_slot(block, p), gu_pair.at[level, p], gu_recv.at[block, p], pair_dev)

    def gu_arrived(block, p):
        remote(gu_slot(block, p), gu_slot(block, p), gu_pair.at[0, 0], gu_recv.at[block, p], pair_dev).wait_recv()

    def down_slot(c, j):
        return down.at[c, pl.ds(pl.multiple_of(j * down_rows, down_rows), down_rows)]

    def down_line_copy(c, up):
        return remote(
            down_slot(c, x), down_slot(c, x), down_line.at[0 if up else 1, c], down_recv.at[x, c],
            {"fs": f + 2 if up else f - 2},
        )

    def down_pair_copy(c):
        return remote(down_slot(c, x), down_slot(c, x), down_pair.at[c], down_recv.at[x, c], pair_dev)

    def down_arrived(c, j):
        remote(down_slot(c, j), down_slot(c, j), down_first, down_recv.at[j, c], pair_dev).wait_recv()

    first_copy = remote(down_in, down_slot(t, x), down_first, down_recv.at[x, t], {"tp": z})
    own_gate = pltpu.make_async_copy(gate_in, gu_slot(f, 0), local.at[0])
    own_up = pltpu.make_async_copy(up_in, gu_slot(f, 1), local.at[3])
    own_tok = pltpu.make_async_copy(tok_in, tok.at[t], local.at[1])
    own_down = pltpu.make_async_copy(down_in, down_slot(t, x), local.at[2])
    tok_near = remote(tok_in, tok.at[t], tok_send.at[0], tok_recv.at[t], {"tp": sibling})
    tok_far = remote(tok_in, tok.at[t], tok_send.at[1], tok_recv.at[t], {"tp": across})
    tok_relay = remote(tok.at[across], tok.at[across], tok_send.at[2], tok_recv.at[across], {"tp": sibling})

    def tok_arrived(s):
        remote(tok.at[s], tok.at[s], tok_send.at[0], tok_recv.at[s], {"tp": sibling}).wait_recv()

    def each_line(step, act):
        for p in range(PIECES):
            for up in (True, False):
                level = z - step if up else z + step

                @pl.when((level >= 0) & (level < lines))
                def _():
                    if act == "start" and step > 0:
                        gu_arrived(2 * level + x, p)

                    @pl.when(z < lines - 1 if up else z > 0)
                    def _():
                        copy = line_copy(step, p, up)
                        copy.start() if act == "start" else copy.wait_send()

                    if step > 0 or up:
                        copy = pair_copy(step, level, p)
                        copy.start() if act == "start" else copy.wait_send()

    def each_down(step, act):
        for k in range(tp):
            c = column(k)

            @pl.when(away == step)
            def _():
                if act == "start":
                    if step == 0:
                        @pl.when(c != t)
                        def _():
                            down_arrived(c, x)
                    else:
                        down_arrived(c, x)

                for up in (True, False):
                    @pl.when((z >= t) & (z < lines - 1) if up else (z <= t) & (z > 0))
                    def _():
                        copy = down_line_copy(c, up)
                        copy.start() if act == "start" else copy.wait_send()

    each_line(0, "start")

    @pl.when(t != z)
    def _():
        first_copy.start()

    tok_far.start()
    tok_near.start()
    own_gate.start()
    own_up.start()
    own_tok.start()

    @pl.when(t == z)
    def _():
        own_down.start()
        own_down.wait()

    for step in range(1, lines):
        each_line(step, "start")
        each_down(step - 1, "start")
        if step == lines // 2:
            tok_arrived(across)
            tok_relay.start()

    @pl.when(away < lines - 1)
    def _():
        for k in range(tp):
            down_pair_copy(column(k)).start()

    own_tok.wait()
    tok_arrived(sibling)
    tok_arrived(3 - t)
    norm_tile = min(128, n_tok)

    def norm_rows(i, carry):
        at = pl.ds(pl.multiple_of(i * norm_tile, norm_tile), norm_tile)
        total = jnp.zeros((norm_tile, 1), jnp.float32)
        for s in range(tp):
            value = tok[s, at, :].astype(jnp.float32)
            total = total + jnp.sum(value * value, axis=-1, keepdims=True)
        scale = lax.rsqrt(total / (tp * width) + norm_eps)
        for s in range(tp):
            normed[at, s * width:(s + 1) * width] = (tok[s, at, :].astype(jnp.float32) * scale).astype(jnp.bfloat16)
        return carry

    lax.fori_loop(0, n_tok // norm_tile, norm_rows, 0)

    own_gate.wait()
    own_up.wait()
    for level in range(lines):
        for p in range(PIECES):
            gu_arrived(2 * level + 1 - x, p)

    def gu_store(block, p):
        return pltpu.make_async_copy(
            gu_slot(block, p), gu_out[p].at[:, block * depth:(block + 1) * depth], stored.at[block, p]
        )

    for block in range(2 * lines):
        for p in range(PIECES):
            gu_store(block, p).start()

    def hidden_rows(i, carry):
        at = pl.ds(pl.multiple_of(i * tile, tile), tile)
        value = normed[at, :]
        gate, up = (
            lax.dot_general(
                value, jnp.concatenate([gu[block, p] for block in range(2 * lines)], axis=1), NT,
                preferred_element_type=jnp.float32,
            )
            for p in range(PIECES)
        )
        hidden[at, :] = (gate / (1.0 + jnp.exp(-gate)) * up).astype(jnp.bfloat16)

        @pl.when(away == lines - 1)
        def _():
            c = column(i)
            down_arrived(c, x)
            down_pair_copy(c).start()

        return carry

    lax.fori_loop(0, tp, hidden_rows, 0)

    def down_store(k):
        c = column(k)
        return pltpu.make_async_copy(
            down.at[c], down_out.at[:, pl.ds(pl.multiple_of(c * width, width), width)], local.at[4 + k]
        )

    sends = [
        remote(part.at[0], got.at[0], sum_send.at[0], sum_recv.at[0], {"tp": sibling}),
        remote(part.at[1], got.at[1], sum_send.at[1], sum_recv.at[1], {"tp": across}),
        remote(part.at[2], got.at[2], sum_send.at[2], sum_recv.at[2], {"tp": sibling}),
    ]
    for k in range(tp):
        c = column(k)
        down_arrived(c, 1 - x)
        down_store(k).start()
        if k == 1:
            sends[0].wait_recv()
        if k == 3:
            sends[2].wait_recv()
            sends[1].wait_recv()

        def part_rows(i, carry):
            at = pl.ds(pl.multiple_of(i * tile, tile), tile)
            value = jnp.dot(hidden[at, :], down[c], preferred_element_type=jnp.float32)
            if k == 1:
                value = value + got[0, at, :].astype(jnp.float32)
            if k == 3:
                value = value + got[2, at, :].astype(jnp.float32) + got[1, at, :].astype(jnp.float32)
                mixed_out[at, :] = value.astype(jnp.bfloat16)
            else:
                part[k, at, :] = value.astype(jnp.bfloat16)
            return carry

        lax.fori_loop(0, tp, part_rows, 0)
        if k < 3:
            sends[k].start()

    for step in range(lines):
        each_line(step, "wait")
    for step in range(lines - 1):
        each_down(step, "wait")
    for k in range(tp):
        down_pair_copy(column(k)).wait_send()
        down_store(k).wait()

    @pl.when(t != z)
    def _():
        first_copy.wait_send()

    tok_near.wait_send()
    tok_far.wait_send()
    tok_relay.wait_send()
    for copy in sends:
        copy.wait_send()
    for block in range(2 * lines):
        for p in range(PIECES):
            gu_store(block, p).wait()


def fused(fs, tp, tokens, gate_local, up_local, down_local):
    lines = fs // 2
    n_tok, width = tokens.shape
    depth, units = gate_local.shape
    down_rows = down_local.shape[0]
    bf16 = jnp.bfloat16
    dma = pltpu.SemaphoreType.DMA
    vmem = pl.BlockSpec(memory_space=pltpu.VMEM)
    anywhere = pl.BlockSpec(memory_space=pl.ANY)
    gate, up, down_sampler, mixed = pl.pallas_call(
        functools.partial(layer_kernel, lines, tp),
        out_shape=(
            jax.ShapeDtypeStruct((units, fs * depth), bf16),
            jax.ShapeDtypeStruct((units, fs * depth), bf16),
            jax.ShapeDtypeStruct((2 * down_rows, tp * width), bf16),
            jax.ShapeDtypeStruct((n_tok, width), bf16),
        ),
        in_specs=[vmem] * 4,
        out_specs=(anywhere, anywhere, anywhere, vmem),
        scratch_shapes=[
            pltpu.VMEM((tp, n_tok, width), bf16),
            pltpu.VMEM((n_tok, tp * width), bf16),
            pltpu.VMEM((fs, PIECES, units, depth), bf16),
            pltpu.VMEM((n_tok, units), bf16),
            pltpu.VMEM((tp, 2 * down_rows, width), bf16),
            pltpu.VMEM((3, n_tok, width), bf16),
            pltpu.VMEM((3, n_tok, width), bf16),
            dma((fs, PIECES)), dma((2, lines, PIECES)), dma((lines, PIECES)),
            dma((2, tp)), dma((2, tp)), dma((tp,)), dma,
            dma((tp,)), dma((3,)), dma((3,)), dma((3,)), dma((4 + tp,)), dma((fs, PIECES)),
        ],
        compiler_params=pltpu.CompilerParams(
            collective_id=0, has_side_effects=True, vmem_limit_bytes=56 * 1024 * 1024
        ),
    )(tokens, gate_local.T, up_local.T, down_local)
    return gate.T, up.T, down_sampler, mixed


def plain(tokens, gate_local, up_local, down_local):
    gathered = lax.all_gather(tokens, "tp", axis=1, tiled=True)
    floated = gathered.astype(jnp.float32)
    normed = (
        floated * lax.rsqrt(jnp.mean(floated * floated, axis=-1, keepdims=True) + norm_eps)
    ).astype(jnp.bfloat16)
    gate_sampler = lax.all_gather(gate_local, "fs", axis=0, tiled=True)
    up_sampler = lax.all_gather(up_local, "fs", axis=0, tiled=True)
    gate = jnp.dot(normed, gate_sampler, preferred_element_type=jnp.float32)
    up = jnp.dot(normed, up_sampler, preferred_element_type=jnp.float32)
    hidden = (jax.nn.silu(gate) * up).astype(jnp.bfloat16)
    down_columns = lax.all_gather(down_local, "fs", axis=0, tiled=True)
    down_sampler = lax.all_to_all(down_columns, "tp", split_axis=0, concat_axis=1, tiled=True)
    mixed = jnp.dot(
        lax.all_gather(hidden, "tp", axis=1, tiled=True), down_columns, preferred_element_type=jnp.float32
    ).astype(jnp.bfloat16)
    return gate_sampler, up_sampler, down_sampler, mixed


def shards(fs, tp, tokens, norm_gain, gate_weight, up_weight, down_weight):
    gate_local = (norm_gain[:, None] * gate_weight).astype(jnp.bfloat16)
    up_local = (norm_gain[:, None] * up_weight).astype(jnp.bfloat16)
    down_local = down_weight.astype(jnp.bfloat16)
    aligned = (
        gate_local.shape[0] % 128 == 0
        and gate_local.shape[1] % 16 == 0
        and down_local.shape[0] % 16 == 0
        and down_local.shape[1] % 128 == 0
        and tokens.shape[0] % (128 * tp) == 0
    )
    if not (tp == 4 and fs == 2 * tp and aligned):
        return plain(tokens, gate_local, up_local, down_local)
    return fused(fs, tp, tokens, gate_local, up_local, down_local)


def solution(mesh):
    return jax.shard_map(
        functools.partial(shards, mesh.shape["fs"], mesh.shape["tp"]),
        mesh=mesh,
        in_specs=(P("fs", "tp"), P("fs"), P("fs", "tp"), P("fs", "tp"), P("fs", "tp")),
        out_specs=(P(None, "tp"), P(None, "tp"), P("tp", None), P("fs", "tp")),
        check_vma=False,
    )
```

time: 317 us -> 142 us (0.45)
  waiting for transfers between devices: 204 us -> 0 us
  Pallas kernels: 0 us -> 127 us
  blocking collectives: 64.5 us -> 0 us
  matrix products: 21.7 us -> 0 us
  between operations: 13.8 us -> 0.65 us
  local copies, waits for them, and re-layouts: 6.45 us -> 9.7 us
    all_gather x5 -> x0, waiting for transfers between devices: 202 us -> none  [the longest x1 59.1 us: shards(): lax.all_gather(gate_local, 'fs', axis=0, tiled=True)]
    pallas_call x0 -> x1, Pallas kernels: none -> 127 us  [fused(): pl.pallas_call(functools.partial(layer_kernel, lines, tp), out_shape=(jax...]
    all_to_all x1 -> x0, blocking collectives: 64.5 us -> none  [shards(): lax.all_to_all(down_columns, 'tp', split_axis=0, concat_axis=1, tiled=True)]
    dot_general x3 -> x0, matrix products: 21.7 us -> none  [the longest x1 7.73 us: shards(): up = jnp.dot(normed, up_sampler, preferred_element_type=jnp.float32)]
    unnamed x8 -> x10, local copies, waits for them, and re-layouts: 4.44 us -> 9.7 us
  transfers between devices with their start and end apart: 5 -> 0, of which waited for: 5 -> 0; matrix products, arithmetic and copies ran while one was open for 7% -> 0% of each run, Pallas kernels for 0% -> 0%
where the time goes in v1:
time: 142 us
  Pallas kernels  127 us (89%)
  local copies, waits for them, and re-layouts  9.7 us (7%)
  other arithmetic  4.2 us (3%)
    pallas_call x1, Pallas kernels, fused(): pl.pallas_call(functools.partial(layer_kernel, lines, tp), out_shape=(jax...  127 us
    unnamed x10, local copies, waits for them, and re-layouts  9.7 us

profile of v1, /device:TPU:0, one launch (start us, length us, event | category | flops | bytes accessed | tf_op | source)
XLA Modules:
  0.0 141.6 jit_solution(4048943767313612463)
XLA Ops:
  0.6 1.9 %convert_element_type.11.down_in = bf16[352,512]{1,0:T(8,128)(2,1)} convert(f32[352,512]{1,0:T(8,128)} %param.9) | non-fusion elementwise | flops 180224 | bytes 1081344 | tf_op jit(solution)/shard_map/convert_element_type | solution.py:349
  2.5 2.3 %fusion.1 = (bf16[704,256]{1,0:T(8,128)(2,1)}, bf16[704,256]{1,0:T(8,128)(2,1)}) fusion(f32[256,704]{0,1:T(8,128)} %param.8, f32[256]{0:T(256)} %param.6, f32[256,704]{0,1:T(8,128)} %param.7), kind=kLoop, calls=%fused_computation.3 | loop fusion | flops 720896 | bytes 2163712 | tf_op jit(solution)/shard_map/transpose | solution.py:323
  4.8 127.0 %shard_map.84 = (bf16[704,2048]{1,0:T(8,128)(2,1)}, bf16[704,2048]{1,0:T(8,128)(2,1)}, bf16[704,2048]{1,0:T(8,128)(2,1)}, bf16[1024,512]{1,0:T(8,128)(2,1)}) custom-call(bf16[1024,512]{1,0:T(8,128)(2,1)} %tok_in.1, bf16[704,256]{1,0:T(8,128)(2,1)} %get-tuple-element.13.gate_in, bf16[704,256]{1,0:T(8,128)(2,1)} %get-tuple-element.12.up_in, ...), custom_call_target="tpu_custom_call" | custom-call | tf_op jit(solution)/shard_map/pallas_call | solution.py:298
  131.9 0.0 copy-start.1
  131.9 3.9 %copy.13 = bf16[2048,704]{0,1:T(8,128)(2,1)} copy(bf16[2048,704]{0,1:T(8,128)(2,1)} %bitcast.7) | data formatting | bytes 5767168
  135.8 0.0 copy-done.1
  135.8 0.0 copy-start
  135.8 1.6 %copy.14 = bf16[2048,704]{0,1:T(8,128)(2,1)} copy(bf16[2048,704]{0,1:T(8,128)(2,1)S(1)} %bitcast.6) | data formatting | bytes 5767168
  137.4 1.3 copy-done
  138.7 0.0 copy-start.2
  138.7 1.6 %copy.15 = bf16[704,2048]{1,0:T(8,128)(2,1)} copy(bf16[704,2048]{1,0:T(8,128)(2,1)S(1)} %copy-done) | data formatting | bytes 5767168
  140.2 0.4 copy-done.2
  140.6 1.0 copy.16
Async XLA Ops:
  131.9 3.9 %copy-start.1 = (bf16[704,2048]{1,0:T(8,128)(2,1)S(1)}, bf16[704,2048]{1,0:T(8,128)(2,1)}, u32[]{:S(2)}) copy-start(bf16[704,2048]{1,0:T(8,128)(2,1)} %get-tuple-element.9) | copy-start | bytes 8650756
  135.8 2.9 %copy-start = (bf16[704,2048]{1,0:T(8,128)(2,1)S(1)}, bf16[704,2048]{1,0:T(8,128)(2,1)}, u32[]{:S(2)}) copy-start(bf16[704,2048]{1,0:T(8,128)(2,1)} %get-tuple-element.20) | copy-start | bytes 8650756
  138.7 2.0 %copy-start.2 = (bf16[1024,512]{1,0:T(8,128)(2,1)S(1)}, bf16[1024,512]{1,0:T(8,128)(2,1)}, u32[]{:S(2)}) copy-start(bf16[1024,512]{1,0:T(8,128)(2,1)} %get-tuple-element.21) | copy-start | bytes 3145732

commit v2 on v1

--- a/solution.py
+++ b/solution.py
@@ -11,6 +11,7 @@
 MESH = pl.DeviceIdType.MESH
 PIECES = 2
 NT = (((1,), (1,)), ((), ()))
+WHOLE = 1
 
 
 def remote(src, dst, send, recv, device):
@@ -80,9 +81,9 @@
     def down_slot(c, j):
         return down.at[c, pl.ds(pl.multiple_of(j * down_rows, down_rows), down_rows)]
 
-    def down_line_copy(c, up):
+    def down_line_copy(c, j, up):
         return remote(
-            down_slot(c, x), down_slot(c, x), down_line.at[0 if up else 1, c], down_recv.at[x, c],
+            down_slot(c, j), down_slot(c, j), down_line.at[0 if up else 1, j, c], down_recv.at[j, c],
             {"fs": f + 2 if up else f - 2},
         )
 
@@ -124,24 +125,27 @@
                         copy.start() if act == "start" else copy.wait_send()
 
     def each_down(step, act):
-        for k in range(tp):
+        for k in (WHOLE,) + tuple(k for k in range(tp) if k != WHOLE):
             c = column(k)
 
             @pl.when(away == step)
             def _():
                 if act == "start":
-                    if step == 0:
+                    if step == 0 and k != WHOLE:
                         @pl.when(c != t)
                         def _():
                             down_arrived(c, x)
-                    else:
+                    if step > 0:
                         down_arrived(c, x)
+                    if k == WHOLE:
+                        down_arrived(c, 1 - x)
 
                 for up in (True, False):
                     @pl.when((z >= t) & (z < lines - 1) if up else (z <= t) & (z > 0))
                     def _():
-                        copy = down_line_copy(c, up)
-                        copy.start() if act == "start" else copy.wait_send()
+                        for j in (x, 1 - x) if k == WHOLE else (x,):
+                            copy = down_line_copy(c, j, up)
+                            copy.start() if act == "start" else copy.wait_send()
 
     each_line(0, "start")
 
@@ -160,17 +164,26 @@
         own_down.start()
         own_down.wait()
 
+    @pl.when(t == z)
+    def _():
+        down_arrived(column(WHOLE), x)
+        down_pair_copy(column(WHOLE)).start()
+
     for step in range(1, lines):
         each_line(step, "start")
-        each_down(step - 1, "start")
+        if step > 1:
+            each_down(step - 2, "start")
         if step == lines // 2:
             tok_arrived(across)
             tok_relay.start()
 
+    each_down(lines - 2, "start")
+
     @pl.when(away < lines - 1)
     def _():
         for k in range(tp):
-            down_pair_copy(column(k)).start()
+            if k != WHOLE:
+                down_pair_copy(column(k)).start()
 
     own_tok.wait()
     tok_arrived(sibling)
@@ -221,7 +234,14 @@
         def _():
             c = column(i)
             down_arrived(c, x)
-            down_pair_copy(c).start()
+
+            @pl.when(i == WHOLE)
+            def _():
+                down_arrived(c, 1 - x)
+
+            @pl.when(i != WHOLE)
+            def _():
+                down_pair_copy(c).start()
 
         return carry
 
@@ -240,7 +260,8 @@
     ]
     for k in range(tp):
         c = column(k)
-        down_arrived(c, 1 - x)
+        if k != WHOLE:
+            down_arrived(c, 1 - x)
         down_store(k).start()
         if k == 1:
             sends[0].wait_recv()
@@ -269,8 +290,13 @@
     for step in range(lines - 1):
         each_down(step, "wait")
     for k in range(tp):
-        down_pair_copy(column(k)).wait_send()
+        if k != WHOLE:
+            down_pair_copy(column(k)).wait_send()
         down_store(k).wait()
+
+    @pl.when(t == z)
+    def _():
+        down_pair_copy(column(WHOLE)).wait_send()
 
     @pl.when(t != z)
     def _():
@@ -314,11 +340,11 @@
             pltpu.VMEM((3, n_tok, width), bf16),
             pltpu.VMEM((3, n_tok, width), bf16),
             dma((fs, PIECES)), dma((2, lines, PIECES)), dma((lines, PIECES)),
-            dma((2, tp)), dma((2, tp)), dma((tp,)), dma,
+            dma((2, tp)), dma((2, 2, tp)), dma((tp,)), dma,
             dma((tp,)), dma((3,)), dma((3,)), dma((3,)), dma((4 + tp,)), dma((fs, PIECES)),
         ],
         compiler_params=pltpu.CompilerParams(
-            collective_id=0, has_side_effects=True, vmem_limit_bytes=56 * 1024 * 1024
+            collective_id=0, has_side_effects=True, vmem_limit_bytes=40 * 1024 * 1024
         ),
     )(tokens, gate_local.T, up_local.T, down_local)
     return gate.T, up.T, down_sampler, mixed

time: 142 us -> 133 us (0.937)
  local copies, waits for them, and re-layouts: 9.7 us -> 5.71 us
  Pallas kernels: 127 us -> 124 us
  other arithmetic: 4.2 us -> 2.7 us
    unnamed x10 -> x6, local copies, waits for them, and re-layouts: 9.7 us -> 5.71 us
    pallas_call x1, Pallas kernels: 127 us -> 124 us  [fused(): pl.pallas_call(functools.partial(layer_kernel, lines, tp), out_shape=(jax...]
where the time goes in v2:
time: 133 us
  Pallas kernels  124 us (93%)
  local copies, waits for them, and re-layouts  5.71 us (4%)
  other arithmetic  2.7 us (2%)
    pallas_call x1, Pallas kernels, fused(): pl.pallas_call(functools.partial(layer_kernel, lines, tp), out_shape=(jax...  124 us
    unnamed x6, local copies, waits for them, and re-layouts  5.71 us

profile of v2, /device:TPU:0, one launch (start us, length us, event | category | flops | bytes accessed | tf_op | source)
XLA Modules:
  0.0 132.8 jit_solution(10180861658728534696)
XLA Ops:
  0.6 0.0 copy-start
  0.6 1.2 convert_element_type.11.down_in
  1.9 1.5 %fusion.1 = (bf16[704,256]{1,0:T(8,128)(2,1)S(1)}, bf16[704,256]{1,0:T(8,128)(2,1)S(1)}) fusion(f32[256,704]{0,1:T(8,128)} %param.8, f32[256]{0:T(256)} %param.6, f32[256,704]{0,1:T(8,128)} %param.7), kind=kLoop, calls=%fused_computation.3 | loop fusion | flops 720896 | bytes 2163712 | tf_op jit(solution)/shard_map/transpose | solution.py:349
  3.4 0.0 copy-done
  3.4 123.7 %shard_map.84 = (bf16[704,2048]{1,0:T(8,128)(2,1)S(1)}, bf16[704,2048]{1,0:T(8,128)(2,1)S(1)}, bf16[704,2048]{1,0:T(8,128)(2,1)S(1)}, bf16[1024,512]{1,0:T(8,128)(2,1)S(1)}) custom-call(bf16[1024,512]{1,0:T(8,128)(2,1)S(1)} %copy-done, bf16[704,256]{1,0:T(8,128)(2,1)S(1)} %get-tuple-element.13.gate_in, bf16[704,256]{1,0:T(8,128)(2,1)S(1)} %get-tuple-element.12.up_in, ...), custom_call_target="tpu_custom_call" | custom-call | tf_op jit(solution)/shard_map/pallas_call | solution.py:324
  127.1 1.6 %copy.13 = bf16[2048,704]{0,1:T(8,128)(2,1)} copy(bf16[2048,704]{0,1:T(8,128)(2,1)S(1)} %bitcast.7) | data formatting | bytes 5767168
  128.6 1.6 %copy.14 = bf16[2048,704]{0,1:T(8,128)(2,1)} copy(bf16[2048,704]{0,1:T(8,128)(2,1)S(1)} %bitcast.6) | data formatting | bytes 5767168
  130.2 1.6 %copy.15 = bf16[704,2048]{1,0:T(8,128)(2,1)} copy(bf16[704,2048]{1,0:T(8,128)(2,1)S(1)} %get-tuple-element.20) | data formatting | bytes 5767168
  131.8 1.0 copy.16
Async XLA Ops:
  0.6 2.7 %copy-start = (bf16[1024,512]{1,0:T(8,128)(2,1)S(1)}, bf16[1024,512]{1,0:T(8,128)(2,1)}, u32[]{:S(2)}) copy-start(bf16[1024,512]{1,0:T(8,128)(2,1)} %tok_in.1) | copy-start | bytes 3145732

commit v3 on v2

--- a/solution.py
+++ b/solution.py
@@ -218,8 +218,26 @@
         for p in range(PIECES):
             gu_store(block, p).start()
 
-    def hidden_rows(i, carry):
-        at = pl.ds(pl.multiple_of(i * tile, tile), tile)
+    def down_store(k):
+        c = column(k)
+        return pltpu.make_async_copy(
+            down.at[c], down_out.at[:, pl.ds(pl.multiple_of(c * width, width), width)], local.at[4 + k]
+        )
+
+    def tile_rows(i):
+        return pl.ds(pl.multiple_of(i * tile, tile), tile)
+
+    def sum_copy(k, i):
+        at = tile_rows(i)
+        return remote(
+            part.at[k, at], got.at[k, at], sum_send.at[k, i], sum_recv.at[k, i], {"tp": across if k == 1 else sibling}
+        )
+
+    def partial(k, at):
+        return jnp.dot(hidden[at, :], down[column(k)], preferred_element_type=jnp.float32)
+
+    def first_rows(i, carry):
+        at = tile_rows(i)
         value = normed[at, :]
         gate, up = (
             lax.dot_general(
@@ -232,58 +250,54 @@
 
         @pl.when(away == lines - 1)
         def _():
-            c = column(i)
-            down_arrived(c, x)
-
-            @pl.when(i == WHOLE)
-            def _():
-                down_arrived(c, 1 - x)
-
             @pl.when(i != WHOLE)
             def _():
-                down_pair_copy(c).start()
-
+                down_arrived(column(i), x)
+                down_pair_copy(column(i)).start()
+
+            @pl.when(i == 0)
+            def _():
+                down_arrived(column(WHOLE), x)
+                down_arrived(column(WHOLE), 1 - x)
+
+        @pl.when(i == 0)
+        def _():
+            down_arrived(column(0), 1 - x)
+            down_store(0).start()
+            down_store(1).start()
+
+        part[0, at, :] = partial(0, at).astype(jnp.bfloat16)
+        value = partial(1, at)
+        sum_copy(0, i).start()
+        sum_copy(0, i).wait_recv()
+        part[1, at, :] = (value + got[0, at, :].astype(jnp.float32)).astype(jnp.bfloat16)
+        sum_copy(1, i).start()
         return carry
 
-    lax.fori_loop(0, tp, hidden_rows, 0)
-
-    def down_store(k):
-        c = column(k)
-        return pltpu.make_async_copy(
-            down.at[c], down_out.at[:, pl.ds(pl.multiple_of(c * width, width), width)], local.at[4 + k]
-        )
-
-    sends = [
-        remote(part.at[0], got.at[0], sum_send.at[0], sum_recv.at[0], {"tp": sibling}),
-        remote(part.at[1], got.at[1], sum_send.at[1], sum_recv.at[1], {"tp": across}),
-        remote(part.at[2], got.at[2], sum_send.at[2], sum_recv.at[2], {"tp": sibling}),
-    ]
-    for k in range(tp):
-        c = column(k)
-        if k != WHOLE:
-            down_arrived(c, 1 - x)
-        down_store(k).start()
-        if k == 1:
-            sends[0].wait_recv()
-        if k == 3:
-            sends[2].wait_recv()
-            sends[1].wait_recv()
-
-        def part_rows(i, carry):
-            at = pl.ds(pl.multiple_of(i * tile, tile), tile)
-            value = jnp.dot(hidden[at, :], down[c], preferred_element_type=jnp.float32)
-            if k == 1:
-                value = value + got[0, at, :].astype(jnp.float32)
-            if k == 3:
-                value = value + got[2, at, :].astype(jnp.float32) + got[1, at, :].astype(jnp.float32)
-                mixed_out[at, :] = value.astype(jnp.bfloat16)
-            else:
-                part[k, at, :] = value.astype(jnp.bfloat16)
-            return carry
-
-        lax.fori_loop(0, tp, part_rows, 0)
-        if k < 3:
-            sends[k].start()
+    lax.fori_loop(0, tp, first_rows, 0)
+    down_arrived(column(2), 1 - x)
+    down_store(2).start()
+
+    def near_rows(i, carry):
+        at = tile_rows(i)
+        part[2, at, :] = partial(2, at).astype(jnp.bfloat16)
+        sum_copy(2, i).start()
+        return carry
+
+    lax.fori_loop(0, tp, near_rows, 0)
+    down_arrived(column(3), 1 - x)
+    down_store(3).start()
+
+    def last_rows(i, carry):
+        at = tile_rows(i)
+        value = partial(3, at)
+        sum_copy(2, i).wait_recv()
+        sum_copy(1, i).wait_recv()
+        value = value + got[2, at, :].astype(jnp.float32) + got[1, at, :].astype(jnp.float32)
+        mixed_out[at, :] = value.astype(jnp.bfloat16)
+        return carry
+
+    lax.fori_loop(0, tp, last_rows, 0)
 
     for step in range(lines):
         each_line(step, "wait")
@@ -305,8 +319,9 @@
     tok_near.wait_send()
     tok_far.wait_send()
     tok_relay.wait_send()
-    for copy in sends:
-        copy.wait_send()
+    for k in range(3):
+        for i in range(tp):
+            sum_copy(k, i).wait_send()
     for block in range(2 * lines):
         for p in range(PIECES):
             gu_store(block, p).wait()
@@ -341,7 +356,7 @@
             pltpu.VMEM((3, n_tok, width), bf16),
             dma((fs, PIECES)), dma((2, lines, PIECES)), dma((lines, PIECES)),
             dma((2, tp)), dma((2, 2, tp)), dma((tp,)), dma,
-            dma((tp,)), dma((3,)), dma((3,)), dma((3,)), dma((4 + tp,)), dma((fs, PIECES)),
+            dma((tp,)), dma((3,)), dma((3, tp)), dma((3, tp)), dma((4 + tp,)), dma((fs, PIECES)),
         ],
         compiler_params=pltpu.CompilerParams(
             collective_id=0, has_side_effects=True, vmem_limit_bytes=40 * 1024 * 1024

time: 133 us -> 130 us (0.977)
  Pallas kernels: 124 us -> 121 us
    pallas_call x1, Pallas kernels: 124 us -> 121 us  [fused(): pl.pallas_call(functools.partial(layer_kernel, lines, tp), out_shape=(jax...]
where the time goes in v3:
time: 130 us
  Pallas kernels  121 us (93%)
  local copies, waits for them, and re-layouts  5.71 us (4%)
  other arithmetic  2.7 us (2%)
    pallas_call x1, Pallas kernels, fused(): pl.pallas_call(functools.partial(layer_kernel, lines, tp), out_shape=(jax...  121 us
    unnamed x6, local copies, waits for them, and re-layouts  5.71 us

profile of v3, /device:TPU:0, one launch (start us, length us, event | category | flops | bytes accessed | tf_op | source)
XLA Modules:
  0.0 129.6 jit_solution(3895433922742753292)
XLA Ops:
  0.6 0.0 copy-start
  0.6 1.2 convert_element_type.11.down_in
  1.9 1.5 %fusion.1 = (bf16[704,256]{1,0:T(8,128)(2,1)S(1)}, bf16[704,256]{1,0:T(8,128)(2,1)S(1)}) fusion(f32[256,704]{0,1:T(8,128)} %param.8, f32[256]{0:T(256)} %param.6, f32[256,704]{0,1:T(8,128)} %param.7), kind=kLoop, calls=%fused_computation.3 | loop fusion | flops 720896 | bytes 2163712 | tf_op jit(solution)/shard_map/transpose | solution.py:364
  3.4 0.0 copy-done
  3.4 120.5 %shard_map.84 = (bf16[704,2048]{1,0:T(8,128)(2,1)S(1)}, bf16[704,2048]{1,0:T(8,128)(2,1)S(1)}, bf16[704,2048]{1,0:T(8,128)(2,1)S(1)}, bf16[1024,512]{1,0:T(8,128)(2,1)S(1)}) custom-call(bf16[1024,512]{1,0:T(8,128)(2,1)S(1)} %copy-done, bf16[704,256]{1,0:T(8,128)(2,1)S(1)} %get-tuple-element.13.gate_in, bf16[704,256]{1,0:T(8,128)(2,1)S(1)} %get-tuple-element.12.up_in, ...), custom_call_target="tpu_custom_call" | custom-call | tf_op jit(solution)/shard_map/pallas_call | solution.py:339
  123.9 1.6 %copy.13 = bf16[2048,704]{0,1:T(8,128)(2,1)} copy(bf16[2048,704]{0,1:T(8,128)(2,1)S(1)} %bitcast.7) | data formatting | bytes 5767168
  125.5 1.6 %copy.14 = bf16[2048,704]{0,1:T(8,128)(2,1)} copy(bf16[2048,704]{0,1:T(8,128)(2,1)S(1)} %bitcast.6) | data formatting | bytes 5767168
  127.0 1.6 %copy.15 = bf16[704,2048]{1,0:T(8,128)(2,1)} copy(bf16[704,2048]{1,0:T(8,128)(2,1)S(1)} %get-tuple-element.20) | data formatting | bytes 5767168
  128.6 1.0 copy.16
Async XLA Ops:
  0.6 2.7 %copy-start = (bf16[1024,512]{1,0:T(8,128)(2,1)S(1)}, bf16[1024,512]{1,0:T(8,128)(2,1)}, u32[]{:S(2)}) copy-start(bf16[1024,512]{1,0:T(8,128)(2,1)} %tok_in.1) | copy-start | bytes 3145732
